TPU v7x, 32 devices: a whole 2x2x4 slice. The times are simulated.
32 devices in a mesh: grp: 2 (over y), fs: 4 (over z), tp: 4 (over x, core).
Axes of the slice: x: 2, y: 2, z: 4, core: 2. Of those that a mesh axis runs over, the one named last changes fastest.
Arguments:
- prompt_rows: bfloat16 [8192, 2048], P(('grp', 'fs')), parts along dimension 0, may hold values from -6 to 6
- up_master: float32 [2048, 8192], P('fs', 'tp'), may hold values from -0.125 to 0.125
- down_master: float32 [8192, 2048], P('fs', 'tp'), may hold values from -0.0625 to 0.0625
- norm_gain: float32 [2048], P('fs'), may hold values from 0.1 to 1.9
Outputs:
- up_sampler: bfloat16 [8, 2048, 2048], P(('grp', 'tp')), parts along dimension 0
- down_sampler: bfloat16 [8, 2048, 2048], P(('grp', 'tp')), parts along dimension 0
- layer_out: bfloat16 [8192, 2048], P(('grp', 'fs', 'tp')), parts along dimension 0
There are 2 independent parts, one for each index of `grp`. A program takes and returns all parts, laid end to end along the dimension named above; an argument that names none is the same for every part. Nothing has to cross between parts.
All inputs are finite; a program needn't handle non-finite values.
Results may differ from a plain program's by a relative error of at most 0.014.
Values may be sent and summed in bfloat16 or wider, within the bound.
A program may use at most 128 MiB of HBM per device.

v0:
```python
import jax
import jax.numpy as jnp
from jax import lax
from jax.sharding import PartitionSpec as P

eps = 1e-06


def on_device(prompt_rows, up_master, down_master, norm_gain):
    fs_count = lax.axis_size("fs")
    tp_count = lax.axis_size("tp")
    fs_per_tp = fs_count // tp_count
    up_cast = (up_master * norm_gain[:, None]).astype(jnp.bfloat16)
    down_cast = down_master.astype(jnp.bfloat16)
    up_local_rows = up_cast.shape[0]
    local_width = up_cast.shape[1]
    unit_span = local_width // fs_count
    down_local_cols = down_cast.shape[1]
    full_width = down_local_cols * tp_count
    values = prompt_rows.astype(jnp.float32)
    normed = (values * lax.rsqrt(jnp.mean(values * values, axis=-1, keepdims=True) + eps)).astype(
        jnp.bfloat16
    )
    up_parts = up_cast.reshape(up_local_rows, fs_per_tp, tp_count, unit_span)
    up_local = lax.all_to_all(up_parts, "tp", split_axis=2, concat_axis=1, tiled=True).reshape(
        up_local_rows, local_width
    )
    up_sampler = lax.all_gather(up_local, "fs", axis=0, tiled=True)
    down_parts = down_cast.reshape(tp_count, unit_span, down_local_cols)
    down_local = lax.all_to_all(down_parts, "tp", split_axis=0, concat_axis=2, tiled=True).reshape(
        unit_span, full_width
    )
    down_sampler = lax.all_gather(down_local, "fs", axis=0, tiled=True)
    pre_act = jnp.dot(normed, up_sampler, preferred_element_type=jnp.float32)
    hidden = jnp.square(jax.nn.relu(pre_act)).astype(jnp.bfloat16)
    summed = lax.psum_scatter(
        jnp.dot(hidden, down_sampler, preferred_element_type=jnp.float32).astype(jnp.bfloat16),
        "tp",
        scatter_dimension=0,
        tiled=True,
    )
    return (up_sampler[None], down_sampler[None], summed)


def solution(mesh):
    in_specs = (P(("grp", "fs"), None), P("fs", "tp"), P("fs", "tp"), P("fs"))
    out_specs = (
        P(("grp", "tp"), None, None),
        P(("grp", "tp"), None, None),
        P(("grp", "fs", "tp"), None),
    )
    return jax.shard_map(
        on_device, mesh=mesh, in_specs=in_specs, out_specs=out_specs, check_vma=False
    )
```

profile of v0, /device:TPU:0, one launch (start us, length us, event | category | flops | bytes accessed | tf_op | source)
XLA Modules:
  0.0 416.7 jit_solution(6983446177385879946)
XLA Ops:
  7.2 0.0 all-gather.5.cloned.1.call-start
  7.2 2.5 convert_element_type.19
  9.7 29.7 %all_to_all.24 = bf16[4,512,512]{2,1,0:T(8,128)(2,1)S(1)} all-to-all(bf16[4,512,512]{2,1,0:T(8,128)(2,1)S(1)} %bitcast.12), channel_id=1, replica_groups=mesh['grp'=2,'fs'=4,'tp'=4] {'tp'}, dimensions={0} | all-to-all | bytes 4194304 | tf_op jit(solution)/shard_map/all_to_all | solution.py:30
  39.4 2.4 copy.11
  41.7 0.0 all-gather.5.cloned.1.call-update
  41.8 0.0 copy-start
  41.8 0.0 all-gather.3.cloned.1.call-start
  41.8 5.3 %copy.8 = f32[512,2048]{0,1:T(8,128)} copy(f32[512,2048]{1,0:T(8,128)} %param.5) | data formatting | bytes 8388608 | tf_op args[1]
  47.2 0.0 copy-done
  47.2 3.1 multiply_convert_fusion.1
  50.3 2.4 copy.9
  52.6 29.3 %all_to_all.25 = bf16[512,1,4,512]{3,0,1,2:T(8,128)(2,1)S(1)} all-to-all(bf16[512,1,4,512]{3,0,1,2:T(8,128)(2,1)} %copy.9), channel_id=1, replica_groups=mesh['grp'=2,'fs'=4,'tp'=4] {'tp'}, dimensions={2} | all-to-all | bytes 4194304 | tf_op jit(solution)/shard_map/all_to_all | solution.py:25
  81.9 2.4 copy.10
  84.3 0.0 all-gather.3.cloned.1.call-update
  84.3 0.0 reduce-scatter.2.cloned.1.call-start
  84.4 3.1 fusion
  87.5 104.3 %all-gather.5.cloned.1.call-done = bf16[2048,2048]{0,1:T(8,128)(2,1)} async-done(((bf16[512,2048]{0,1:T(8,128)(2,1)}), bf16[2048,2048]{0,1:T(8,128)(2,1)}) %all-gather.5.cloned.1.call-update) | async-done | bytes 8388624 | tf_op jit(solution)/shard_map/all_gather | solution.py:33
  191.8 150.0 %all-gather.3.cloned.1.call-done = bf16[2048,2048]{0,1:T(8,128)(2,1)} async-done(((bf16[512,2048]{0,1:T(8,128)(2,1)}), bf16[2048,2048]{0,1:T(8,128)(2,1)}) %all-gather.3.cloned.1.call-update) | async-done | bytes 8388624 | tf_op jit(solution)/shard_map/all_gather | solution.py:28
  341.8 25.4 %fusion.9 = bf16[1024,2048]{1,0:T(8,128)(2,1)} fusion(bf16[2048,2048]{0,1:T(8,128)(2,1)} %all-gather.5.cloned.1.call-done, bf16[2048,2048]{0,1:T(8,128)(2,1)} %all-gather.3.cloned.1.call-done, bf16[1024,2048]{1,0:T(8,128)(2,1)} %param.4, f32[1024]{0:T(1024)S(1)} %add_rsqrt_fusion), kind=kOutput, calls=%fused_computation.9 | convolution fusion | flops 17194549248 | bytes 25169920 | tf_op jit(solution)/shard_map/dot_general | solution.py:37
  367.2 0.0 reduce-scatter.2.cloned.1.call-update
  367.3 12.3 %copy.12 = bf16[1,2048,2048]{2,1,0:T(8,128)(2,1)} copy(bf16[1,2048,2048]{1,2,0:T(8,128)(2,1)} %bitcast.14) | data formatting | bytes 16777216
  379.6 12.0 %copy.13 = bf16[1,2048,2048]{2,1,0:T(8,128)(2,1)} copy(bf16[1,2048,2048]{1,2,0:T(8,128)(2,1)} %bitcast.13) | data formatting | bytes 16777216
  391.5 18.6 %reduce-scatter.2.cloned.1.call-done = bf16[256,2048]{1,0:T(8,128)(2,1)} async-done(((bf16[1024,2048]{1,0:T(8,128)(2,1)}), bf16[256,2048]{1,0:T(8,128)(2,1)}) %reduce-scatter.2.cloned.1.call-update) | async-done | bytes 1048592 | tf_op jit(solution)/shard_map/reduce_scatter | solution.py:36
  (1 shorter events, 0.0 us)
Async XLA Ops:
  7.2 184.7 %all-gather.5.cloned.1.call-start = ((), (), s32[]{:S(2)}) async-start(), calls=%async_computation.4 | async-start | bytes 10485760 | tf_op jit(solution)/shard_map/all_gather | solution.py:33
  41.8 5.4 %copy-start = (f32[512]{0:T(512)S(1)}, f32[512]{0:T(512)}, u32[]{:S(2)}) copy-start(f32[512]{0:T(512)} %param.7) | copy-start | bytes 6148
  41.8 300.0 %all-gather.3.cloned.1.call-start = ((), (), s32[]{:S(2)}) async-start(), calls=%async_computation.3 | async-start | bytes 10485760 | tf_op jit(solution)/shard_map/all_gather | solution.py:28
  84.3 325.9 %reduce-scatter.2.cloned.1.call-start = ((), (), s32[]{:S(2)}) async-start(), calls=%async_computation.5 | async-start | bytes 5242880 | tf_op jit(solution)/shard_map/reduce_scatter | solution.py:36
Sparse Core Ops, SparseCore 0:
  41.9 149.9 all-gather.4
  194.0 147.7 all-gather.2
  367.4 42.7 reduce-scatter.1
where the time goes:
time: 418 us; the launch traced here: 417 us
  waiting for transfers between devices  273 us (65%)
  blocking collectives  59 us (14%)
  local copies, waits for them, and re-layouts  36.7 us (9%)
  matrix products  25.4 us (6%)
  between operations  13.8 us (3%)
  other arithmetic  8.69 us (2%)
    all_gather x1, waiting for transfers between devices, on_device(): up_sampler = lax.all_gather(up_local, 'fs', axis=0, tiled=True)  150 us
    all_gather x1, waiting for transfers between devices, on_device(): down_sampler = lax.all_gather(down_local, 'fs', axis=0, tiled=True)  104 us
    all_to_all x1, blocking collectives, on_device(): lax.all_to_all(down_parts, 'tp', split_axis=0, concat_axis=2, tiled=True)  29.7 us
    unnamed x5, local copies, waits for them, and re-layouts  29.7 us
    all_to_all x1, blocking collectives, on_device(): lax.all_to_all(up_parts, 'tp', split_axis=2, concat_axis=1, tiled=True)  29.3 us
    dot_general x1, matrix products, on_device(): jnp.dot(hidden, down_sampler, preferred_element_type=jnp.float32)  25.4 us
    reduce_scatter x1, waiting for transfers between devices, on_device(): lax.psum_scatter(jnp.dot(hidden, down_sampler, preferred_element_type=jnp...  18.6 us
  transfers between devices with their start and end apart: 3, of which 3 were waited for; matrix products, arithmetic and copies ran while one was open for 10% of the time, Pallas kernels for 0%

commit v1 on v0

--- a/solution.py
+++ b/solution.py
@@ -30,7 +30,9 @@
     down_local = lax.all_to_all(down_parts, "tp", split_axis=0, concat_axis=2, tiled=True).reshape(
         unit_span, full_width
     )
-    down_sampler = lax.all_gather(down_local, "fs", axis=0, tiled=True)
+    down_sampler = jnp.concatenate(
+        lax.all_to_all(jnp.stack([down_local] * lax.axis_size("fs")), "fs", 0, 0), axis=0
+    )
     pre_act = jnp.dot(normed, up_sampler, preferred_element_type=jnp.float32)
     hidden = jnp.square(jax.nn.relu(pre_act)).astype(jnp.bfloat16)
     summed = lax.psum_scatter(

time: 418 us -> 489 us (1.17)
  waiting for transfers between devices: 273 us -> 378 us
  blocking collectives: 59 us -> 0 us
  starting transfers between devices: 0.12 us -> 14.7 us
  local copies, waits for them, and re-layouts: 36.7 us -> 44.2 us
    all_gather x1, waiting for transfers between devices: 150 us -> 294 us  [on_device(): up_sampler = lax.all_gather(up_local, 'fs', axis=0, tiled=True)]
    all_gather x1 -> x0, waiting for transfers between devices: 104 us -> none  [on_device(): down_sampler = lax.all_gather(down_local, 'fs', axis=0, tiled=True)]
    all_to_all x2 -> x0, blocking collectives: 59 us -> none  [the longest x1 29.7 us: on_device(): lax.all_to_all(down_parts, 'tp', split_axis=0, concat_axis=2, tiled=True)]
    all_to_all x0 -> x3, waiting for transfers between devices: none -> 53.6 us  [the longest x1 21.1 us: on_device(): lax.all_to_all(jnp.stack([down_local] * lax.axis_size('fs')), 'fs', 0, 0)]
    all_to_all x0 -> x3, starting transfers between devices: none -> 14.5 us  [the longest x1 5.79 us: on_device(): lax.all_to_all(jnp.stack([down_local] * lax.axis_size('fs')), 'fs', 0, 0)]
    reduce_scatter x1, waiting for transfers between devices: 18.6 us -> 30.7 us  [on_device(): lax.psum_scatter(jnp.dot(hidden, down_sampler, preferred_element_type=jnp...]
  transfers between devices with their start and end apart: 3 -> 5, of which waited for: 3 -> 5; matrix products, arithmetic and copies ran while one was open for 10% -> 8% of each run, Pallas kernels for 0% -> 0%
where the time goes in v1:
time: 489 us; the launch traced here: 488 us
  waiting for transfers between devices  378 us (77%)
  local copies, waits for them, and re-layouts  44.2 us (9%)
  matrix products  25.6 us (5%)
  starting transfers between devices  14.7 us (3%)
  between operations  14.1 us (3%)
  other arithmetic  11.3 us (2%)
    all_gather x1, waiting for transfers between devices, on_device(): up_sampler = lax.all_gather(up_local, 'fs', axis=0, tiled=True)  294 us
    reduce_scatter x1, waiting for transfers between devices, on_device(): lax.psum_scatter(jnp.dot(hidden, down_sampler, preferred_element_type=jnp...  30.7 us
    unnamed x5, local copies, waits for them, and re-layouts  26.1 us
    dot_general x1, matrix products, on_device(): jnp.dot(hidden, down_sampler, preferred_element_type=jnp.float32)  25.6 us
    all_to_all x1, waiting for transfers between devices, on_device(): lax.all_to_all(jnp.stack([down_local] * lax.axis_size('fs')), 'fs', 0, 0)  21.1 us
    all_to_all x1, waiting for transfers between devices, on_device(): lax.all_to_all(up_parts, 'tp', split_axis=2, concat_axis=1, tiled=True)  20.4 us
    all_to_all x1, waiting for transfers between devices, on_device(): lax.all_to_all(down_parts, 'tp', split_axis=0, concat_axis=2, tiled=True)  12.1 us
  transfers between devices with their start and end apart: 5, of which 5 were waited for; matrix products, arithmetic and copies ran while one was open for 8% of the time, Pallas kernels for 0%

profile of v1, /device:TPU:0, one launch (start us, length us, event | category | flops | bytes accessed | tf_op | source)
XLA Modules:
  0.0 488.0 jit_solution(8762681000412079163)
XLA Ops:
  7.2 3.8 convert_element_type.19
  11.0 4.2 all-to-all-start.1
  15.2 5.3 %copy.12 = f32[512,2048]{0,1:T(8,128)} copy(f32[512,2048]{1,0:T(8,128)} %param.5) | data formatting | bytes 8388608 | tf_op args[1]
  20.6 4.1 multiply_convert_fusion.1
  24.6 4.1 copy.13
  28.8 12.1 %all-to-all-done.1 = bf16[4,512,512]{2,1,0:T(8,128)(2,1)S(1)} async-done(((bf16[4,512,512]{2,1,0:T(8,128)(2,1)}), bf16[4,512,512]{2,1,0:T(8,128)(2,1)S(1)}, u32[]{:S(2)}, u32[]{:S(2)}) %all-to-all-start.1) | async-done | bytes 2097184 | tf_op jit(solution)/shard_map/all_to_all | solution.py:30
  40.9 4.4 all-to-all-start
  45.3 0.0 all-gather.2.cloned.1.call-start
  45.4 2.4 copy.15
  47.7 2.9 copy.16
  50.7 20.4 %all-to-all-done = bf16[512,1,4,512]{3,0,1,2:T(8,128)(2,1)} async-done(((bf16[512,1,4,512]{3,0,1,2:T(8,128)(2,1)}), bf16[512,1,4,512]{3,0,1,2:T(8,128)(2,1)}, u32[]{:S(2)}, u32[]{:S(2)}) %all-to-all-start) | async-done | bytes 2097184 | tf_op jit(solution)/shard_map/all_to_all | solution.py:25
  71.1 4.1 copy.14
  75.2 0.0 all-gather.2.cloned.1.call-update
  75.2 4.5 stack.3
  79.7 5.8 %all-to-all-start.2 = ((bf16[4,512,2048]{2,1,0:T(8,128)(2,1)}), bf16[4,512,2048]{2,1,0:T(8,128)(2,1)}, u32[]{:S(2)}, u32[]{:S(2)}) async-start(bf16[4,512,2048]{2,1,0:T(8,128)(2,1)} %stack.3), calls=%async_computation.2 | async-start | bytes 16777216 | tf_op jit(solution)/shard_map/all_to_all | solution.py:34
  85.5 0.2 reduce-scatter.2.cloned.1.call-start
  85.7 3.4 fusion
  89.1 293.9 %all-gather.2.cloned.1.call-done = bf16[2048,2048]{0,1:T(8,128)(2,1)} async-done(((bf16[512,2048]{0,1:T(8,128)(2,1)}), bf16[2048,2048]{0,1:T(8,128)(2,1)}) %all-gather.2.cloned.1.call-update) | async-done | bytes 8388624 | tf_op jit(solution)/shard_map/all_gather | solution.py:28
  383.0 21.1 %all-to-all-done.2 = bf16[4,512,2048]{2,1,0:T(8,128)(2,1)} async-done(((bf16[4,512,2048]{2,1,0:T(8,128)(2,1)}), bf16[4,512,2048]{2,1,0:T(8,128)(2,1)}, u32[]{:S(2)}, u32[]{:S(2)}) %all-to-all-start.2) | async-done | bytes 8388640 | tf_op jit(solution)/shard_map/all_to_all | solution.py:34
  404.1 25.6 %fusion.9 = bf16[1024,2048]{1,0:T(8,128)(2,1)} fusion(bf16[2048,2048]{1,0:T(8,128)(2,1)} %bitcast.8, bf16[2048,2048]{0,1:T(8,128)(2,1)} %all-gather.2.cloned.1.call-done, bf16[1024,2048]{1,0:T(8,128)(2,1)} %param.4, f32[1024]{0:T(1024)S(1)} %add_rsqrt_fusion), kind=kOutput, calls=%fused_computation.9 | convolution fusion | flops 17194549248 | bytes 25169920 | tf_op jit(solution)/shard_map/dot_general | solution.py:39
  429.7 0.0 reduce-scatter.2.cloned.1.call-update
  429.7 12.4 %copy.17 = bf16[1,2048,2048]{2,1,0:T(8,128)(2,1)} copy(bf16[1,2048,2048]{1,2,0:T(8,128)(2,1)} %bitcast.12) | data formatting | bytes 16777216
  442.1 30.7 %reduce-scatter.2.cloned.1.call-done = bf16[256,2048]{1,0:T(8,128)(2,1)} async-done(((bf16[1024,2048]{1,0:T(8,128)(2,1)}), bf16[256,2048]{1,0:T(8,128)(2,1)}) %reduce-scatter.2.cloned.1.call-update) | async-done | bytes 1048592 | tf_op jit(solution)/shard_map/reduce_scatter | solution.py:38
  472.8 8.4 %copy.19 = bf16[1,2048,2048]{2,1,0:T(8,128)(2,1)} copy(bf16[1,2048,2048]{2,1,0:T(8,128)(2,1)} %bitcast.7) | data formatting | bytes 16777216
  (3 shorter events, 0.0 us)
Async XLA Ops:
  11.0 29.9 %all-to-all-start.1 = ((bf16[4,512,512]{2,1,0:T(8,128)(2,1)}), bf16[4,512,512]{2,1,0:T(8,128)(2,1)S(1)}, u32[]{:S(2)}, u32[]{:S(2)}) async-start(bf16[4,512,512]{2,1,0:T(8,128)(2,1)} %bitcast.3), calls=%async_computation.1 | async-start | bytes 4194304 | tf_op jit(solution)/shard_map/all_to_all | solution.py:30
  15.2 5.4 %copy-start = (f32[512]{0:T(512)S(1)}, f32[512]{0:T(512)}, u32[]{:S(2)}) copy-start(f32[512]{0:T(512)} %param.7) | copy-start | bytes 6148
  40.9 30.2 %all-to-all-start = ((bf16[512,1,4,512]{3,0,1,2:T(8,128)(2,1)}), bf16[512,1,4,512]{3,0,1,2:T(8,128)(2,1)}, u32[]{:S(2)}, u32[]{:S(2)}) async-start(bf16[512,1,4,512]{3,0,1,2:T(8,128)(2,1)} %copy.13), calls=%async_computation | async-start | bytes 4194304 | tf_op jit(solution)/shard_map/all_to_all | solution.py:25
  45.3 337.7 %all-gather.2.cloned.1.call-start = ((), (), s32[]{:S(2)}) async-start(), calls=%async_computation.4 | async-start | bytes 10485760 | tf_op jit(solution)/shard_map/all_gather | solution.py:28
  79.7 324.4 %all-to-all-start.2 = ((bf16[4,512,2048]{2,1,0:T(8,128)(2,1)}), bf16[4,512,2048]{2,1,0:T(8,128)(2,1)}, u32[]{:S(2)}, u32[]{:S(2)}) async-start(bf16[4,512,2048]{2,1,0:T(8,128)(2,1)} %stack.3), calls=%async_computation.2 | async-start | bytes 16777216 | tf_op jit(solution)/shard_map/all_to_all | solution.py:34
  85.5 387.3 %reduce-scatter.2.cloned.1.call-start = ((), (), s32[]{:S(2)}) async-start(), calls=%async_computation.5 | async-start | bytes 5242880 | tf_op jit(solution)/shard_map/reduce_scatter | solution.py:38
Sparse Core Ops, SparseCore 0:
  75.3 307.6 all-gather.1
  429.9 42.8 reduce-scatter.1

commit v2 on v0

--- a/solution.py
+++ b/solution.py
@@ -25,12 +25,15 @@
     up_local = lax.all_to_all(up_parts, "tp", split_axis=2, concat_axis=1, tiled=True).reshape(
         up_local_rows, local_width
     )
-    up_sampler = lax.all_gather(up_local, "fs", axis=0, tiled=True)
     down_parts = down_cast.reshape(tp_count, unit_span, down_local_cols)
     down_local = lax.all_to_all(down_parts, "tp", split_axis=0, concat_axis=2, tiled=True).reshape(
         unit_span, full_width
     )
-    down_sampler = lax.all_gather(down_local, "fs", axis=0, tiled=True)
+    up_sampler, down_sampler = jnp.split(
+        lax.all_gather(jnp.concatenate([up_local, down_local], axis=1), "fs", axis=0, tiled=True),
+        [up_local.shape[1]],
+        axis=1,
+    )
     pre_act = jnp.dot(normed, up_sampler, preferred_element_type=jnp.float32)
     hidden = jnp.square(jax.nn.relu(pre_act)).astype(jnp.bfloat16)
     summed = lax.psum_scatter(

time: 418 us -> 443 us (1.060)
  blocking collectives: 59 us -> 0 us
  waiting for transfers between devices: 273 us -> 326 us
  local copies, waits for them, and re-layouts: 36.7 us -> 53 us
  starting transfers between devices: 0.12 us -> 8.77 us
  other arithmetic: 8.69 us -> 14.8 us
    all_to_all x2 -> x0, blocking collectives: 59 us -> none  [the longest x1 29.7 us: on_device(): lax.all_to_all(down_parts, 'tp', split_axis=0, concat_axis=2, tiled=True)]
    all_to_all x0 -> x2, waiting for transfers between devices: none -> 35.4 us  [the longest x1 23.3 us: on_device(): lax.all_to_all(up_parts, 'tp', split_axis=2, concat_axis=1, tiled=True)]
    all_gather x2 -> x1, waiting for transfers between devices: 254 us -> 285 us  [on_device(): lax.all_gather(jnp.concatenate([up_local, down_local], axis=1), 'fs', axi...]
    reduce_scatter x1, waiting for transfers between devices: 18.6 us -> 5.96 us  [on_device(): lax.psum_scatter(jnp.dot(hidden, down_sampler, preferred_element_type=jnp...]
    broadcast_in_dim x0 -> x1, local copies, waits for them, and re-layouts: none -> 12.5 us  [on_device(): return (up_sampler[None], down_sampler[None], summed)]
    all_to_all x0 -> x2, starting transfers between devices: none -> 8.69 us  [the longest x1 4.45 us: on_device(): lax.all_to_all(up_parts, 'tp', split_axis=2, concat_axis=1, tiled=True)]
    unnamed x5 -> x7, local copies, waits for them, and re-layouts: 29.7 us -> 29.8 us
  transfers between devices with their start and end apart: 3 -> 4, of which waited for: 3 -> 4; matrix products, arithmetic and copies ran while one was open for 10% -> 13% of each run, Pallas kernels for 0% -> 0%
where the time goes in v2:
time: 443 us; the launch traced here: 442 us
  waiting for transfers between devices  326 us (74%)
  local copies, waits for them, and re-layouts  53 us (12%)
  matrix products  25.1 us (6%)
  other arithmetic  14.8 us (3%)
  between operations  14.1 us (3%)
  starting transfers between devices  8.77 us (2%)
    all_gather x1, waiting for transfers between devices, on_device(): lax.all_gather(jnp.concatenate([up_local, down_local], axis=1), 'fs', axi...  285 us
    unnamed x7, local copies, waits for them, and re-layouts  29.8 us
    dot_general x1, matrix products, on_device(): jnp.dot(hidden, down_sampler, preferred_element_type=jnp.float32)  25.1 us
    all_to_all x1, waiting for transfers between devices, on_device(): lax.all_to_all(up_parts, 'tp', split_axis=2, concat_axis=1, tiled=True)  23.3 us
    broadcast_in_dim x1, local copies, waits for them, and re-layouts, on_device(): return (up_sampler[None], down_sampler[None], summed)  12.5 us
    all_to_all x1, waiting for transfers between devices, on_device(): lax.all_to_all(down_parts, 'tp', split_axis=0, concat_axis=2, tiled=True)  12.1 us
  transfers between devices with their start and end apart: 4, of which 4 were waited for; matrix products, arithmetic and copies ran while one was open for 13% of the time, Pallas kernels for 0%

profile of v2, /device:TPU:0, one launch (start us, length us, event | category | flops | bytes accessed | tf_op | source)
XLA Modules:
  0.0 442.0 jit_solution(1620309905507870245)
XLA Ops:
  7.2 3.8 convert_element_type.19
  10.9 4.2 all-to-all-start.1
  15.2 5.3 %copy.8 = f32[512,2048]{0,1:T(8,128)} copy(f32[512,2048]{1,0:T(8,128)} %param.5) | data formatting | bytes 8388608 | tf_op args[1]
  20.5 0.0 copy-done.1
  20.5 4.1 multiply_convert_fusion.1
  24.6 4.1 copy.9
  28.7 12.1 %all-to-all-done.1 = bf16[4,512,512]{2,1,0:T(8,128)(2,1)S(1)} async-done(((bf16[4,512,512]{2,1,0:T(8,128)(2,1)}), bf16[4,512,512]{2,1,0:T(8,128)(2,1)S(1)}, u32[]{:S(2)}, u32[]{:S(2)}) %all-to-all-start.1) | async-done | bytes 2097184 | tf_op jit(solution)/shard_map/all_to_all | solution.py:29
  40.9 4.5 %all-to-all-start = ((bf16[512,1,4,512]{3,0,1,2:T(8,128)(2,1)}), bf16[512,1,4,512]{3,0,1,2:T(8,128)(2,1)}, u32[]{:S(2)}, u32[]{:S(2)}) async-start(bf16[512,1,4,512]{3,0,1,2:T(8,128)(2,1)} %copy.9), calls=%async_computation | async-start | bytes 4194304 | tf_op jit(solution)/shard_map/all_to_all | solution.py:25
  45.3 0.0 all-gather.2.cloned.1.call-start
  45.4 2.4 copy.11
  47.7 23.3 %all-to-all-done = bf16[512,1,4,512]{3,0,1,2:T(8,128)(2,1)} async-done(((bf16[512,1,4,512]{3,0,1,2:T(8,128)(2,1)}), bf16[512,1,4,512]{3,0,1,2:T(8,128)(2,1)}, u32[]{:S(2)}, u32[]{:S(2)}) %all-to-all-start) | async-done | bytes 2097184 | tf_op jit(solution)/shard_map/all_to_all | solution.py:25
  71.0 4.1 copy.10
  75.2 0.0 copy-done
  75.2 3.9 pad_maximum_fusion
  79.0 0.0 all-gather.2.cloned.1.call-update
  79.1 0.0 reduce-scatter.2.cloned.1.call-start
  79.1 3.1 fusion
  82.2 284.9 %all-gather.2.cloned.1.call-done = bf16[2048,4096]{0,1:T(8,128)(2,1)} async-done(((bf16[512,4096]{0,1:T(8,128)(2,1)}), bf16[2048,4096]{0,1:T(8,128)(2,1)}) %all-gather.2.cloned.1.call-update) | async-done | bytes 16777232 | tf_op jit(solution)/shard_map/all_gather | solution.py:33
  367.1 25.1 %fusion.10 = bf16[1024,2048]{1,0:T(8,128)(2,1)} fusion(bf16[2048,4096]{0,1:T(8,128)(2,1)} %all-gather.2.cloned.1.call-done, bf16[1024,2048]{1,0:T(8,128)(2,1)} %param.4, f32[1024]{0:T(1024)S(1)} %add_rsqrt_fusion), kind=kOutput, calls=%fused_computation.14 | convolution fusion | flops 17194549248 | bytes 25169920 | tf_op jit(solution)/shard_map/dot_general | solution.py:40
  392.2 0.0 reduce-scatter.2.cloned.1.call-update
  392.2 12.5 %slice_bitcast_fusion = (bf16[1,2048,2048]{1,2,0:T(8,128)(2,1)}, bf16[1,2048,2048]{1,2,0:T(8,128)(2,1)}) fusion(bf16[2048,4096]{0,1:T(8,128)(2,1)} %all-gather.2.cloned.1.call-done), kind=kLoop, calls=%fused_computation.7 | loop fusion | bytes 33554432 | tf_op jit(solution)/shard_map/broadcast_in_dim | solution.py:45
  404.7 12.2 %copy.13 = bf16[1,2048,2048]{2,1,0:T(8,128)(2,1)} copy(bf16[1,2048,2048]{1,2,0:T(8,128)(2,1)} %get-tuple-element.6) | data formatting | bytes 16777216
  416.9 12.2 %copy.12 = bf16[1,2048,2048]{2,1,0:T(8,128)(2,1)} copy(bf16[1,2048,2048]{1,2,0:T(8,128)(2,1)} %get-tuple-element.7) | data formatting | bytes 16777216
  429.2 6.0 %reduce-scatter.2.cloned.1.call-done = bf16[256,2048]{1,0:T(8,128)(2,1)} async-done(((bf16[1024,2048]{1,0:T(8,128)(2,1)}), bf16[256,2048]{1,0:T(8,128)(2,1)}) %reduce-scatter.2.cloned.1.call-update) | async-done | bytes 1048592 | tf_op jit(solution)/shard_map/reduce_scatter | solution.py:39
  (3 shorter events, 0.0 us)
Async XLA Ops:
  10.9 29.9 %all-to-all-start.1 = ((bf16[4,512,512]{2,1,0:T(8,128)(2,1)}), bf16[4,512,512]{2,1,0:T(8,128)(2,1)S(1)}, u32[]{:S(2)}, u32[]{:S(2)}) async-start(bf16[4,512,512]{2,1,0:T(8,128)(2,1)} %bitcast.2), calls=%async_computation.1 | async-start | bytes 4194304 | tf_op jit(solution)/shard_map/all_to_all | solution.py:29
  15.2 5.4 %copy-start.1 = (f32[512]{0:T(512)S(1)}, f32[512]{0:T(512)}, u32[]{:S(2)}) copy-start(f32[512]{0:T(512)} %param.7) | copy-start | bytes 6148
  40.9 30.2 %all-to-all-start = ((bf16[512,1,4,512]{3,0,1,2:T(8,128)(2,1)}), bf16[512,1,4,512]{3,0,1,2:T(8,128)(2,1)}, u32[]{:S(2)}, u32[]{:S(2)}) async-start(bf16[512,1,4,512]{3,0,1,2:T(8,128)(2,1)} %copy.9), calls=%async_computation | async-start | bytes 4194304 | tf_op jit(solution)/shard_map/all_to_all | solution.py:25
  45.3 321.8 %all-gather.2.cloned.1.call-start = ((), (), s32[]{:S(2)}) async-start(), calls=%async_computation.3 | async-start | bytes 20971520 | tf_op jit(solution)/shard_map/all_gather | solution.py:33
  47.7 27.4 %copy-start = (bf16[4,512,512]{1,2,0:T(8,128)(2,1)S(1)}, bf16[4,512,512]{1,2,0:T(8,128)(2,1)}, u32[]{:S(2)}) copy-start(bf16[4,512,512]{1,2,0:T(8,128)(2,1)} %copy.11) | copy-start | bytes 6291460
  79.1 356.1 %reduce-scatter.2.cloned.1.call-start = ((), (), s32[]{:S(2)}) async-start(), calls=%async_computation.4 | async-start | bytes 5242880 | tf_op jit(solution)/shard_map/reduce_scatter | solution.py:39
Sparse Core Ops, SparseCore 0:
  79.2 287.8 all-gather.1
  392.3 42.7 reduce-scatter.1
